TPU v7x, 32 devices: a whole 2x2x4 slice. The times are simulated.
32 devices in a mesh: sp: 8 (over z, x), tp: 4 (over y, core).
Axes of the slice: x: 2, y: 2, z: 4, core: 2. Of those that a mesh axis runs over, the one named last changes fastest.
Arguments:
- stream: bfloat16 [4096, 2048], P(('sp', 'tp')), may hold values from -6 to 6
- queries: bfloat16 [4096, 512], P('sp', 'tp'), may hold values from -6 to 6
- key_rows: bfloat16 [4096, 512], P('sp', 'tp'), may hold values from -6 to 6
- values: bfloat16 [4096, 1024], P('sp', 'tp'), may hold values from -6 to 6
- out_gate: bfloat16 [4096, 1024], P('sp', 'tp'), may hold values from -6 to 6
- fwd_decay: float32 [4096, 512], P('sp', 'tp'), may hold values from -14 to 14
- bwd_decay: float32 [4096, 512], P('sp', 'tp'), may hold values from -14 to 14
- head_gain: float32 [1024], P('tp'), may hold values from 0.1 to 1.9
- out_proj: bfloat16 [1024, 2048], replicated, may hold values from -0.1875 to 0.1875
- mix_gain: float32 [2048], replicated, may hold values from 0.1 to 1.9
- ffn_gain: float32 [2048], replicated, may hold values from 0.1 to 1.9
- moe_gain: float32 [2048], replicated, may hold values from 0.1 to 1.9
- routes: int32 [4096, 2], P(('sp', 'tp')), may hold values from 0 to 7, all different within a row; in each aligned block of 128 rows (0 to 127, 128 to 255, ...) at most 48 rows name the same one
- route_weight: float32 [4096, 2], P(('sp', 'tp')), may hold values from 0.25 to 2.5
- expert_gate: bfloat16 [8, 2048, 1024], P('sp', None, 'tp'), may hold values from -0.125 to 0.125
- expert_up: bfloat16 [8, 2048, 1024], P('sp', None, 'tp'), may hold values from -0.125 to 0.125
- expert_down: bfloat16 [8, 1024, 2048], P('sp', 'tp'), may hold values from -0.1875 to 0.1875
- shared_gate: bfloat16 [2048, 512], P(None, 'tp'), may hold values from -0.125 to 0.125
- shared_up: bfloat16 [2048, 512], P(None, 'tp'), may hold values from -0.125 to 0.125
- shared_down: bfloat16 [512, 2048], P('tp'), may hold values from -0.25 to 0.25
Outputs:
- updated: bfloat16 [4096, 2048], P(('sp', 'tp'))
Inputs may be any that keep to these rules, and one draw needn't show every extreme that they name: `routes`: each row names 2 different experts. Among the rows of one device no expert is named more than 48 times, and in every draw some device names some expert exactly 48 times.
All inputs are finite; a program needn't handle non-finite values.
Results may differ from a plain program's by a relative error of at most 0.023.
Values may be sent and summed in bfloat16 or wider, within the bound.
A program may use at most 128 MiB of HBM per device.

v0:
```python
import jax
import jax.numpy as jnp
from jax import lax
from jax.sharding import PartitionSpec as P

KEY_CHANNELS = 64
DV = 128
BLK = 64
TOPK = 2
EPS = 1e-06
GATE_NORM = 16.0
ROPE_BASE = 10000.0
TOP_PRECISION = lax.Precision.HIGHEST


def carried_in(fwd_summary, bwd_summary, axis):
    count = lax.axis_size(axis)
    place = lax.axis_index(axis)
    decays = jnp.stack([fwd_summary[0], bwd_summary[0]])
    states = jnp.stack([fwd_summary[1], bwd_summary[1]])
    width = states.shape[-1]
    packed = jnp.concatenate([states.reshape(-1, width), decays.reshape(-1, width)], axis=0).astype(
        jnp.bfloat16
    )
    gathered = lax.all_gather(packed, axis).astype(jnp.float32)
    state_rows = states.size // width
    all_states = gathered[:, :state_rows].reshape((count,) + states.shape)
    all_decays = gathered[:, state_rows:].reshape((count,) + decays.shape)
    fwd = jnp.zeros_like(states[0])
    bwd = jnp.zeros_like(states[0])
    for step in range(count):
        fwd = jnp.where(
            step < place, fwd * all_decays[step, 0][:, :, None] + all_states[step, 0], fwd
        )
        source = count - 1 - step
        bwd = jnp.where(
            source > place, bwd * all_decays[source, 1][:, :, None] + all_states[source, 1], bwd
        )
    return (fwd, bwd)


def normalize(tensor):
    return tensor * lax.rsqrt(jnp.mean(tensor * tensor, axis=-1, keepdims=True) + EPS)


def rotate(tensor, positions):
    half_width = tensor.shape[-1] // 2
    frequency = ROPE_BASE ** (-jnp.arange(half_width, dtype=jnp.float32) / half_width)
    angles = positions[:, None] * frequency[None, :]
    cosine = jnp.cos(angles)[:, None, :]
    sine_part = jnp.sin(angles)[:, None, :]
    front_half = tensor[..., :half_width]
    back_half = tensor[..., half_width:]
    return jnp.concatenate(
        [front_half * cosine - back_half * sine_part, front_half * sine_part + back_half * cosine],
        axis=-1,
    )


def blockwise(query_rows, key_data, value_matrix, log_decay, start_state):
    length, head_count, key_width = query_rows.shape
    value_width = value_matrix.shape[-1]
    block_count = length // BLK
    query_blocks = query_rows.reshape(block_count, BLK, head_count, key_width)
    key_blocks = key_data.reshape(block_count, BLK, head_count, key_width)
    value_blocks = value_matrix.reshape(block_count, BLK, head_count, value_width)
    cumul = jnp.cumsum(log_decay.reshape(block_count, BLK, head_count, key_width), axis=1)
    middle = cumul[:, BLK // 2 - 1 : BLK // 2]
    query_scaled = query_blocks * jnp.exp(cumul - middle)
    key_scaled = key_blocks * jnp.exp(middle - cumul)
    scores = jnp.einsum("nthk,nshk->nhts", query_scaled, key_scaled, precision=TOP_PRECISION)
    lower_mask = jnp.arange(BLK)[:, None] >= jnp.arange(BLK)[None, :]
    scores = jnp.where(lower_mask, scores, 0.0)
    within = jnp.einsum("nhts,nshv->nthv", scores, value_blocks, precision=TOP_PRECISION)
    last_cumul = cumul[:, -1:]
    query_in = query_blocks * jnp.exp(cumul)
    key_out = key_blocks * jnp.exp(last_cumul - cumul)
    block_decay = jnp.exp(last_cumul[:, 0])

    def advance(carried_state, pieces):
        query_segment, key_segment, value_segment, decay_segment = pieces
        across_blocks = jnp.einsum(
            "asu,sun->asn", query_segment, carried_state, precision=TOP_PRECISION
        )
        carried_state = carried_state * decay_segment[:, :, None] + jnp.einsum(
            "jco,jcm->com", key_segment, value_segment, precision=TOP_PRECISION
        )
        return (carried_state, across_blocks)

    final_state, across_blocks = lax.scan(
        advance, start_state, (query_in, key_out, value_blocks, block_decay), unroll=block_count
    )
    return ((within + across_blocks).reshape(length, head_count, value_width), final_state)


def summarize(key_data, value_matrix, log_decay):
    cumul = jnp.cumsum(log_decay, axis=0)
    grand_total = cumul[-1]
    weighted_rows = key_data * jnp.exp(grand_total[None] - cumul)
    return (
        jnp.exp(grand_total),
        jnp.einsum("jco,jcm->com", weighted_rows, value_matrix, precision=TOP_PRECISION),
    )


def feed_forward(row_data, gate_parts, up_parts, down_mat):
    groups, _, width = gate_parts.shape
    total = jnp.zeros((row_data.shape[0], down_mat.shape[1]), jnp.float32)
    for group in range(groups):
        hidden = (
            jax.nn.silu(jnp.dot(row_data, gate_parts[group], preferred_element_type=jnp.float32))
            * jnp.dot(row_data, up_parts[group], preferred_element_type=jnp.float32)
        ).astype(jnp.bfloat16)
        total = total + jnp.dot(
            hidden,
            down_mat[group * width : (group + 1) * width],
            preferred_element_type=jnp.float32,
        )
    return total


def slot_map(route_block, experts, capacity):
    tokens, choices = route_block.shape
    flat_ids = route_block.reshape(-1)
    total = flat_ids.shape[0]
    onehot = (flat_ids[:, None] == jnp.arange(experts, dtype=jnp.int32)[None, :]).astype(
        jnp.bfloat16
    )
    earlier = (jnp.arange(total)[:, None] > jnp.arange(total)[None, :]).astype(jnp.bfloat16)
    before = jnp.dot(earlier, onehot, preferred_element_type=jnp.float32)
    slot_ids = jnp.sum(before * onehot.astype(jnp.float32), axis=1).astype(jnp.int32)
    return (flat_ids * capacity + slot_ids).reshape(tokens, choices)


def body(
    stream,
    queries,
    key_rows,
    values,
    out_gate,
    fwd_decay,
    bwd_decay,
    head_gain,
    out_proj,
    mix_gain,
    ffn_gain,
    moe_gain,
    routes,
    route_weight,
    expert_gate,
    expert_up,
    expert_down,
    shared_gate,
    shared_up,
    shared_down,
):
    tokens_here = stream.shape[0]
    span_rows = queries.shape[0]
    heads_here = queries.shape[1] // KEY_CHANNELS
    experts = lax.axis_size("sp")
    capacity = max(2, 3 * tokens_here * TOPK // (2 * experts))
    gate_parts = lax.all_gather(expert_gate[0], "tp")
    up_parts = lax.all_gather(expert_up[0], "tp")
    down_mat = lax.all_gather(expert_down[0], "tp", axis=0, tiled=True)
    shared_gate_parts = lax.all_gather(shared_gate, "tp")
    shared_up_parts = lax.all_gather(shared_up, "tp")
    shared_down_mat = lax.all_gather(shared_down, "tp", axis=0, tiled=True)
    rows_of = slot_map(routes, experts, capacity)
    slots = jnp.arange(experts * capacity, dtype=jnp.int32)
    taken = rows_of[:, :, None] == slots[None, None, :]
    pick = jnp.any(taken, axis=1).astype(jnp.bfloat16)
    weights = jnp.sum(jnp.where(taken, route_weight[:, :, None], 0.0), axis=1)
    weights_high = weights.astype(jnp.bfloat16)
    weights_low = (weights - weights_high.astype(jnp.float32)).astype(jnp.bfloat16)
    offset = lax.axis_index("sp") * span_rows
    positions = (offset + jnp.arange(span_rows, dtype=jnp.int32)).astype(jnp.float32)
    query_rows = rotate(
        queries.astype(jnp.float32).reshape(span_rows, heads_here, KEY_CHANNELS)
        * KEY_CHANNELS ** (-0.5),
        positions,
    )
    key_data = rotate(
        key_rows.astype(jnp.float32).reshape(span_rows, heads_here, KEY_CHANNELS), positions
    )
    value_matrix = values.astype(jnp.float32).reshape(span_rows, heads_here, DV)
    fwd_log = jax.nn.log_sigmoid(fwd_decay).reshape(span_rows, heads_here, KEY_CHANNELS) / GATE_NORM
    bwd_log = (
        jax.nn.log_sigmoid(bwd_decay[::-1]).reshape(span_rows, heads_here, KEY_CHANNELS) / GATE_NORM
    )
    query_back = query_rows[::-1]
    key_back = key_data[::-1]
    value_back = value_matrix[::-1]
    fwd_summary = summarize(key_data, value_matrix, fwd_log)
    bwd_summary = summarize(key_back, value_back, bwd_log)
    fwd_carry, bwd_carry = carried_in(fwd_summary, bwd_summary, "sp")
    fwd_out, _ = blockwise(query_rows, key_data, value_matrix, fwd_log, fwd_carry)
    bwd_out, _ = blockwise(query_back, key_back, value_back, bwd_log, bwd_carry)
    combined = normalize(fwd_out + bwd_out[::-1]) * head_gain.reshape(heads_here, DV)
    head_mixed = (
        combined.reshape(span_rows, -1) * jax.nn.silu(out_gate.astype(jnp.float32))
    ).astype(jnp.bfloat16)
    mixed_out = lax.all_to_all(head_mixed, "tp", split_axis=0, concat_axis=1, tiled=True)
    projected = jnp.dot(mixed_out, out_proj, preferred_element_type=jnp.float32)
    residual = (stream.astype(jnp.float32) + normalize(projected) * mix_gain).astype(jnp.bfloat16)
    normed = (normalize(residual.astype(jnp.float32)) * ffn_gain).astype(jnp.bfloat16)
    model_width = normed.shape[1]
    outgoing = lax.dot_general(
        pick, normed, (((0,), (0,)), ((), ())), preferred_element_type=jnp.float32
    ).astype(jnp.bfloat16)
    arrived = lax.all_to_all(
        outgoing.reshape(experts, capacity, model_width),
        "sp",
        split_axis=0,
        concat_axis=0,
        tiled=True,
    )
    shared_sum = feed_forward(normed, shared_gate_parts, shared_up_parts, shared_down_mat)
    routed_done = feed_forward(
        arrived.reshape(experts * capacity, model_width), gate_parts, up_parts, down_mat
    ).astype(jnp.bfloat16)
    routed_back = lax.all_to_all(
        routed_done.reshape(experts, capacity, model_width),
        "sp",
        split_axis=0,
        concat_axis=0,
        tiled=True,
    ).reshape(experts * capacity, model_width)
    mixture = (
        shared_sum
        + jnp.dot(weights_high, routed_back, preferred_element_type=jnp.float32)
        + jnp.dot(weights_low, routed_back, preferred_element_type=jnp.float32)
    )
    return (residual.astype(jnp.float32) + normalize(mixture) * moe_gain).astype(jnp.bfloat16)


def solution(mesh):
    return jax.shard_map(
        body,
        mesh=mesh,
        in_specs=(
            P(("sp", "tp"), None),
            P("sp", "tp"),
            P("sp", "tp"),
            P("sp", "tp"),
            P("sp", "tp"),
            P("sp", "tp"),
            P("sp", "tp"),
            P("tp"),
            P(),
            P(),
            P(),
            P(),
            P(("sp", "tp"), None),
            P(("sp", "tp"), None),
            P("sp", None, "tp"),
            P("sp", None, "tp"),
            P("sp", "tp", None),
            P(None, "tp"),
            P(None, "tp"),
            P("tp", None),
        ),
        out_specs=P(("sp", "tp"), None),
        check_vma=False,
    )
```

profile of v0, /device:TPU:0, one launch (start us, length us, event | category | flops | bytes accessed | tf_op | source)
XLA Modules:
  0.0 286.0 jit_solution(18210130579138707508)
XLA Ops:
  11.9 2.4 reduce-window.14
  17.0 2.4 reduce-window.16
  22.3 3.8 %rev.17 = f32[512,2,128]{0,2,1:T(8,128)S(1)} reverse(f32[512,2,128]{0,2,1:T(8,128)} %bitcast.614), dimensions={0} | reverse | bytes 1048576 | tf_op jit(solution)/shard_map/rev | solution.py:192
  29.0 33.1 %all_gather.28 = bf16[8,258,128]{2,1,0:T(8,128)(2,1)S(1)} all-gather(bf16[1,258,128]{2,1,0:T(8,128)(2,1)S(1)} %pad_maximum_fusion.2), channel_id=1, replica_groups=mesh['sp'=8,'tp'=4] {'sp'}, dimensions={0}, use_global_device_ids=true | all-gather | bytes 594432 | tf_op jit(solution)/shard_map/all_gather | solution.py:25
  71.4 3.3 %rev.18 = f32[512,2,64]{0,2,1:T(8,128)} reverse(f32[512,2,64]{0,2,1:T(8,128)} %get-tuple-element.71), dimensions={0} | reverse | bytes 524288 | tf_op jit(solution)/shard_map/rev | solution.py:190
  75.1 13.0 %fusion.218 = f32[8,64,2,64]{3,0,1,2:T(8,128)S(1)} fusion(f32[8,64,2,64]{3,0,1,2:T(8,128)S(1)} %copy.390), kind=kOutput, calls=%fused_computation.394 | output fusion | flops 4128768 | bytes 524288 | tf_op jit(solution)/shard_map/jit(cumsum)/reduce_window_sum | solution.py:67
  95.8 1.6 fusion.215
  99.2 1.6 fusion.216
  107.6 2.2 copy_multiply_fusion.1
  138.2 1.7 fusion.11
  140.9 1.7 fusion.10
  143.6 1.7 fusion.9
  146.5 1.7 fusion
  150.6 3.4 %all-to-all-start = ((bf16[4,128,256]{2,1,0:T(8,128)(2,1)}), bf16[4,128,256]{2,1,0:T(8,128)(2,1)S(1)}, u32[]{:S(2)}, u32[]{:S(2)}) async-start(bf16[4,128,256]{2,1,0:T(8,128)(2,1)} %bitcast.143), calls=%async_computation | async-start | bytes 524288 | tf_op jit(solution)/shard_map/all_to_all | solution.py:202
  155.5 4.6 %all-to-all-done = bf16[4,128,256]{2,1,0:T(8,128)(2,1)S(1)} async-done(((bf16[4,128,256]{2,1,0:T(8,128)(2,1)}), bf16[4,128,256]{2,1,0:T(8,128)(2,1)S(1)}, u32[]{:S(2)}, u32[]{:S(2)}) %all-to-all-start) | async-done | bytes 262176 | tf_op jit(solution)/shard_map/all_to_all | solution.py:202
  160.2 3.1 %multiply_reduce_fusion.1 = (f32[128]{0:T(128)S(1)}, f32[128,2048]{1,0:T(8,128)S(1)}) fusion(bf16[128,1024]{0,1:T(8,128)(2,1)S(1)} %bitcast.616, bf16[1024,2048]{1,0:T(8,128)(2,1)} %param.28), kind=kOutput, calls=%fused_computation.110 | convolution fusion | flops 537395072 | bytes 5505536 | tf_op jit(solution)/shard_map/dot_general | solution.py:203
  164.0 1.8 convolution_convert_fusion
  165.8 5.6 %all-to-all-start.1 = ((bf16[8,48,2048]{2,1,0:T(8,128)(2,1)}), bf16[8,48,2048]{2,1,0:T(8,128)(2,1)S(1)}, u32[]{:S(2)}, u32[]{:S(2)}) async-start(bf16[8,48,2048]{2,1,0:T(8,128)(2,1)} %bitcast.608), calls=%async_computation.1 | async-start | bytes 3145728 | tf_op jit(solution)/shard_map/all_to_all | solution.py:210
  172.0 36.1 %all-to-all-done.1 = bf16[8,48,2048]{2,1,0:T(8,128)(2,1)S(1)} async-done(((bf16[8,48,2048]{2,1,0:T(8,128)(2,1)}), bf16[8,48,2048]{2,1,0:T(8,128)(2,1)S(1)}, u32[]{:S(2)}, u32[]{:S(2)}) %all-to-all-start.1) | async-done | bytes 1572896 | tf_op jit(solution)/shard_map/all_to_all | solution.py:210
  208.1 1.9 fusion.39
  211.9 5.0 %fusion.7 = f32[384,2048]{1,0:T(8,128)} fusion(bf16[384,2048]{1,0:T(8,128)(2,1)S(1)} %bitcast.600, bf16[1,1024,2048]{2,1,0:T(8,128)(2,1)} %all-gather.20.cloned.1.call-done, bf16[4,2048,256]{2,1,0:T(8,128)(2,1)} %all-gather.14.cloned.1.call-done, f32[384,256]{1,0:T(8,128)S(1)} %fusion.39), kind=kOutput, calls=%fused_computation.25 | convolution fusion | flops 805896192 | bytes 7208960 | tf_op jit(solution)/shard_map/dot_general | solution.py:114
  216.8 1.8 fusion.37
  218.6 5.0 %fusion.8 = f32[384,2048]{1,0:T(8,128)} fusion(bf16[384,2048]{1,0:T(8,128)(2,1)S(1)} %bitcast.602, bf16[1,1024,2048]{2,1,0:T(8,128)(2,1)} %all-gather.20.cloned.1.call-done, bf16[4,2048,256]{2,1,0:T(8,128)(2,1)} %all-gather.14.cloned.1.call-done, f32[384,256]{1,0:T(8,128)S(1)} %fusion.40), kind=kOutput, calls=%fused_computation.26 | convolution fusion | flops 805896192 | bytes 7208960 | tf_op jit(solution)/shard_map/dot_general | solution.py:114
  223.7 5.0 %fusion.6 = f32[384,2048]{1,0:T(8,128)} fusion(bf16[384,2048]{1,0:T(8,128)(2,1)S(1)} %bitcast.603, bf16[1,1024,2048]{2,1,0:T(8,128)(2,1)} %all-gather.20.cloned.1.call-done, bf16[4,2048,256]{2,1,0:T(8,128)(2,1)} %all-gather.14.cloned.1.call-done, f32[384,256]{1,0:T(8,128)S(1)} %fusion.38), kind=kOutput, calls=%fused_computation.24 | convolution fusion | flops 805896192 | bytes 7208960 | tf_op jit(solution)/shard_map/dot_general | solution.py:114
  228.6 7.3 %add_convert_fusion = bf16[384,2048]{1,0:T(8,128)(2,1)} fusion(f32[384,2048]{1,0:T(8,128)} %fusion.6, f32[384,2048]{1,0:T(8,128)} %fusion.8, f32[384,2048]{1,0:T(8,128)} %fusion.7, bf16[1,1024,2048]{2,1,0:T(8,128)(2,1)} %all-gather.20.cloned.1.call-done, bf16[384,2048]{1,0:T(8,128)(2,1)S(1)} %bitcast.604, ...), kind=kOutput, calls=%fused_computation | convolution fusion | flops 809041920 | bytes 15073280 | tf_op jit(solution)/shard_map/dot_general | solution.py:114
  236.0 4.0 %all-to-all-start.2 = ((bf16[8,48,2048]{2,1,0:T(8,128)(2,1)}), bf16[8,48,2048]{2,1,0:T(8,128)(2,1)S(1)}, u32[]{:S(2)}, u32[]{:S(2)}) async-start(bf16[8,48,2048]{2,1,0:T(8,128)(2,1)} %bitcast.607), calls=%async_computation.2 | async-start | bytes 3145728 | tf_op jit(solution)/shard_map/all_to_all | solution.py:221
  240.1 1.5 fusion.48
  244.5 1.8 fusion.31
  246.3 2.8 convolution_add_fusion.4
  249.1 3.2 %convolution_add_fusion.3 = f32[128,2048]{1,0:T(8,128)} fusion(f32[128,2048]{1,0:T(8,128)} %convolution_add_fusion.4, bf16[512,2048]{1,0:T(8,128)(2,1)} %all-gather.10.cloned.1.call-done, bf16[8192,128]{1,0:T(8,128)(2,1)} %all-gather.18.cloned.1.call-done, f32[128,128]{1,0:T(8,128)S(1)} %fusion.53, bf16[128,2048]{1,0:T(8,128)(2,1)S(1)} %get-tuple-element.6, ...), kind=kOutput, calls=%fused_computation.5 | convolution fusion | flops 135626752 | bytes 3744256 | tf_op jit(solution)/shard_map/dot_general | solution.py:114
  252.3 2.1 convolution_add_fusion.2
  254.4 22.5 %all-to-all-done.2 = bf16[8,48,2048]{2,1,0:T(8,128)(2,1)S(1)} async-done(((bf16[8,48,2048]{2,1,0:T(8,128)(2,1)}), bf16[8,48,2048]{2,1,0:T(8,128)(2,1)S(1)}, u32[]{:S(2)}, u32[]{:S(2)}) %all-to-all-start.2) | async-done | bytes 1572896 | tf_op jit(solution)/shard_map/all_to_all | solution.py:221
  (321 shorter events, 82.1 us)
Async XLA Ops:
  6.5 201.6 %all-gather.12.cloned.1.call-start = ((), (), s32[]{:S(2)}) async-start(), calls=%async_computation.4 | async-start | bytes 5242880 | tf_op jit(solution)/shard_map/all_gather | solution.py:162
  7.3 204.6 %all-gather.14.cloned.1.call-start = ((), (), s32[]{:S(2)}) async-start(), calls=%async_computation.5 | async-start | bytes 5242880 | tf_op jit(solution)/shard_map/all_gather | solution.py:163
  8.0 203.8 %all-gather.20.cloned.1.call-start = ((), (), s32[]{:S(2)}) async-start(), calls=%async_computation.8 | async-start | bytes 5242880 | tf_op jit(solution)/shard_map/all_gather | solution.py:164
  8.7 231.4 %all-gather.16.cloned.1.call-start = ((), (), s32[]{:S(2)}) async-start(), calls=%async_computation.6 | async-start | bytes 2621440 | tf_op jit(solution)/shard_map/all_gather | solution.py:165
  106.2 9.2 %copy-start.26 = (bf16[8,2,8,128]{3,2,1,0:T(8,128)(2,1)S(1)}, bf16[8,2,8,128]{3,2,1,0:T(8,128)(2,1)}, u32[]{:S(2)}) copy-start(bf16[8,2,8,128]{3,2,1,0:T(8,128)(2,1)} %get-tuple-element.22) | copy-start | bytes 98308
  106.2 9.2 %copy-start.48 = (f32[1,2,64]{2,0,1:T(1,128)S(1)}, f32[1,2,64]{2,0,1:T(1,128)}, u32[]{:S(2)}) copy-start(f32[1,2,64]{2,0,1:T(1,128)} %get-tuple-element.55) | copy-start | bytes 1540
  107.5 25.7 %copy-start.4 = (f32[8,64,2,64]{3,1,2,0:T(8,128)}, f32[8,64,2,64]{3,1,2,0:T(8,128)S(1)}, u32[]{:S(2)}) copy-start(f32[8,64,2,64]{3,1,2,0:T(8,128)S(1)} %fusion.65) | copy-start | bytes 786436
  107.5 10.0 %copy-start.25 = (bf16[8,2,8,128]{3,2,1,0:T(8,128)(2,1)S(1)}, bf16[8,2,8,128]{3,2,1,0:T(8,128)(2,1)}, u32[]{:S(2)}) copy-start(bf16[8,2,8,128]{3,2,1,0:T(8,128)(2,1)} %get-tuple-element.21) | copy-start | bytes 98308
  107.5 10.0 %copy-start.47 = (f32[1,2,64]{2,0,1:T(1,128)S(1)}, f32[1,2,64]{2,0,1:T(1,128)}, u32[]{:S(2)}) copy-start(f32[1,2,64]{2,0,1:T(1,128)} %get-tuple-element.54) | copy-start | bytes 1540
  107.5 12.1 %copy-start.24 = (bf16[8,2,8,128]{3,2,1,0:T(8,128)(2,1)S(1)}, bf16[8,2,8,128]{3,2,1,0:T(8,128)(2,1)}, u32[]{:S(2)}) copy-start(bf16[8,2,8,128]{3,2,1,0:T(8,128)(2,1)} %get-tuple-element.20) | copy-start | bytes 98308
  107.6 12.1 %copy-start.46 = (f32[1,2,64]{2,0,1:T(1,128)S(1)}, f32[1,2,64]{2,0,1:T(1,128)}, u32[]{:S(2)}) copy-start(f32[1,2,64]{2,0,1:T(1,128)} %get-tuple-element.53) | copy-start | bytes 1540
  107.6 14.2 %copy-start.23 = (bf16[8,2,8,128]{3,2,1,0:T(8,128)(2,1)S(1)}, bf16[8,2,8,128]{3,2,1,0:T(8,128)(2,1)}, u32[]{:S(2)}) copy-start(bf16[8,2,8,128]{3,2,1,0:T(8,128)(2,1)} %get-tuple-element.25) | copy-start | bytes 98308
  107.6 14.2 %copy-start.45 = (f32[1,2,64]{2,0,1:T(1,128)S(1)}, f32[1,2,64]{2,0,1:T(1,128)}, u32[]{:S(2)}) copy-start(f32[1,2,64]{2,0,1:T(1,128)} %get-tuple-element.52) | copy-start | bytes 1540
  109.8 14.0 %copy-start.22 = (bf16[8,2,8,128]{3,2,1,0:T(8,128)(2,1)S(1)}, bf16[8,2,8,128]{3,2,1,0:T(8,128)(2,1)}, u32[]{:S(2)}) copy-start(bf16[8,2,8,128]{3,2,1,0:T(8,128)(2,1)} %get-tuple-element.19) | copy-start | bytes 98308
  109.8 14.0 %copy-start.44 = (f32[1,2,64]{2,0,1:T(1,128)S(1)}, f32[1,2,64]{2,0,1:T(1,128)}, u32[]{:S(2)}) copy-start(f32[1,2,64]{2,0,1:T(1,128)} %get-tuple-element.51) | copy-start | bytes 1540
  109.8 16.2 %copy-start.52 = (f32[2,64]{1,0:T(2,128)S(1)}, f32[2,64]{1,0:T(2,128)}, u32[]{:S(2)}) copy-start(f32[2,64]{1,0:T(2,128)} %get-tuple-element.36) | copy-start | bytes 1540
  109.8 16.2 %copy-start.53 = (f32[2,64]{1,0:T(2,128)S(1)}, f32[2,64]{1,0:T(2,128)}, u32[]{:S(2)}) copy-start(f32[2,64]{1,0:T(2,128)} %get-tuple-element.37) | copy-start | bytes 1540
  109.8 16.2 %copy-start.54 = (f32[2,64]{1,0:T(2,128)S(1)}, f32[2,64]{1,0:T(2,128)}, u32[]{:S(2)}) copy-start(f32[2,64]{1,0:T(2,128)} %get-tuple-element.38) | copy-start | bytes 1540
  109.8 16.2 %copy-start.55 = (f32[2,64]{1,0:T(2,128)S(1)}, f32[2,64]{1,0:T(2,128)}, u32[]{:S(2)}) copy-start(f32[2,64]{1,0:T(2,128)} %get-tuple-element.39) | copy-start | bytes 1540
  109.8 16.2 %copy-start.56 = (f32[2,64]{1,0:T(2,128)S(1)}, f32[2,64]{1,0:T(2,128)}, u32[]{:S(2)}) copy-start(f32[2,64]{1,0:T(2,128)} %get-tuple-element.40) | copy-start | bytes 1540
  109.9 16.2 %copy-start.57 = (f32[2,64]{1,0:T(2,128)S(1)}, f32[2,64]{1,0:T(2,128)}, u32[]{:S(2)}) copy-start(f32[2,64]{1,0:T(2,128)} %get-tuple-element.41) | copy-start | bytes 1540
  109.9 16.2 %copy-start.58 = (f32[2,64]{1,0:T(2,128)S(1)}, f32[2,64]{1,0:T(2,128)}, u32[]{:S(2)}) copy-start(f32[2,64]{1,0:T(2,128)} %get-tuple-element.42) | copy-start | bytes 1540
  109.9 16.2 %copy-start.59 = (f32[2,64]{1,0:T(2,128)S(1)}, f32[2,64]{1,0:T(2,128)}, u32[]{:S(2)}) copy-start(f32[2,64]{1,0:T(2,128)} %get-tuple-element.43) | copy-start | bytes 1540
  110.2 16.9 %copy-start.7 = (f32[8,64,2,64]{1,3,2,0:T(8,128)S(1)}, f32[8,64,2,64]{1,3,2,0:T(8,128)}, u32[]{:S(2)}) copy-start(f32[8,64,2,64]{1,3,2,0:T(8,128)} %copy.400) | copy-start | bytes 786436
  117.5 9.8 %copy-start.20 = (f32[64,2,128]{2,0,1:T(8,128)S(1)}, f32[64,2,128]{2,0,1:T(8,128)}, u32[]{:S(2)}) copy-start(f32[64,2,128]{2,0,1:T(8,128)} %slice.528) | copy-start | bytes 196612
  117.5 9.8 %copy-start.43 = (f32[1,2,64]{2,0,1:T(1,128)S(1)}, f32[1,2,64]{2,0,1:T(1,128)}, u32[]{:S(2)}) copy-start(f32[1,2,64]{2,0,1:T(1,128)} %get-tuple-element.64) | copy-start | bytes 1540
  134.6 10.7 %copy-start.32 = (f32[8,2,64]{2,0,1:T(8,128)S(1)}, f32[8,2,64]{2,0,1:T(8,128)}, u32[]{:S(2)}) copy-start(f32[8,2,64]{2,0,1:T(8,128)} %get-tuple-element.13) | copy-start | bytes 12292
  150.6 9.4 %all-to-all-start = ((bf16[4,128,256]{2,1,0:T(8,128)(2,1)}), bf16[4,128,256]{2,1,0:T(8,128)(2,1)S(1)}, u32[]{:S(2)}, u32[]{:S(2)}) async-start(bf16[4,128,256]{2,1,0:T(8,128)(2,1)} %bitcast.143), calls=%async_computation | async-start | bytes 524288 | tf_op jit(solution)/shard_map/all_to_all | solution.py:202
  154.0 90.4 %all-gather.10.cloned.1.call-start = ((), (), s32[]{:S(2)}) async-start(), calls=%async_computation.3 | async-start | bytes 2621440 | tf_op jit(solution)/shard_map/all_gather | solution.py:167
  165.8 42.3 %all-to-all-start.1 = ((bf16[8,48,2048]{2,1,0:T(8,128)(2,1)}), bf16[8,48,2048]{2,1,0:T(8,128)(2,1)S(1)}, u32[]{:S(2)}, u32[]{:S(2)}) async-start(bf16[8,48,2048]{2,1,0:T(8,128)(2,1)} %bitcast.608), calls=%async_computation.1 | async-start | bytes 3145728 | tf_op jit(solution)/shard_map/all_to_all | solution.py:210
  171.4 73.0 %all-gather.18.cloned.1.call-start = ((), (), s32[]{:S(2)}) async-start(), calls=%async_computation.7 | async-start | bytes 2621440 | tf_op jit(solution)/shard_map/all_gather | solution.py:166
  236.0 41.0 %all-to-all-start.2 = ((bf16[8,48,2048]{2,1,0:T(8,128)(2,1)}), bf16[8,48,2048]{2,1,0:T(8,128)(2,1)S(1)}, u32[]{:S(2)}, u32[]{:S(2)}) async-start(bf16[8,48,2048]{2,1,0:T(8,128)(2,1)} %bitcast.607), calls=%async_computation.2 | async-start | bytes 3145728 | tf_op jit(solution)/shard_map/all_to_all | solution.py:221
  (50 other events, 235.0 us)
Sparse Core Ops, SparseCore 0:
  8.9 37.2 all-gather.11
  47.7 34.4 all-gather.13
  83.7 34.4 all-gather.19
  119.6 22.5 all-gather.15
  156.1 24.0 all-gather.9
  181.6 22.5 all-gather.17
where the time goes:
time: 288 us; the launch traced here: 286 us
  matrix products  83 us (29%)
  waiting for transfers between devices  66.7 us (23%)
  local copies, waits for them, and re-layouts  42.4 us (15%)
  blocking collectives  33.1 us (11%)
  other arithmetic  32.2 us (11%)
  between operations  15.1 us (5%)
  starting transfers between devices  13.4 us (5%)
    all_to_all x1, waiting for transfers between devices, body(): lax.all_to_all(outgoing.reshape(experts, capacity, model_width), 'sp', sp...  36.1 us
    all_gather x1, blocking collectives, carried_in(): gathered = lax.all_gather(packed, axis).astype(jnp.float32)  33.1 us
    dot_general x8, matrix products, feed_forward(): jnp.dot(hidden, down_mat[group * width:(group + 1) * width], preferred_el...  32.3 us
    all_to_all x1, waiting for transfers between devices, body(): lax.all_to_all(routed_done.reshape(experts, capacity, model_width), 'sp',...  22.5 us
    dot_general x16, matrix products, advance(): jnp.einsum('asu,sun->asn', query_segment, carried_state, precision=TOP_PR...  17.6 us
    another operation x2, other arithmetic, blockwise(): jnp.cumsum(log_decay.reshape(block_count, BLK, head_count, key_width), ax...  14.1 us
    dot_general x14, matrix products, advance(): jnp.einsum('jco,jcm->com', key_segment, value_segment, precision=TOP_PREC...  10.9 us
    slice x17, local copies, waits for them, and re-layouts, blockwise(): lax.scan(advance, start_state, (query_in, key_out, value_blocks, block_de...  9.6 us
  transfers between devices with their start and end apart: 9, of which 3 were waited for; matrix products, arithmetic and copies ran while one was open for 54% of the time, Pallas kernels for 0%

commit v1 on v0

--- a/solution.py
+++ b/solution.py
@@ -11,6 +11,13 @@
 GATE_NORM = 16.0
 ROPE_BASE = 10000.0
 TOP_PRECISION = lax.Precision.HIGHEST
+
+
+def task_drive(inputs):
+    return jnp.concatenate(
+        lax.all_to_all(jnp.stack(jnp.split(inputs, lax.axis_size("tp"), axis=0)), "tp", 0, 0),
+        axis=1,
+    )
 
 
 def carried_in(fwd_summary, bwd_summary, axis):
@@ -199,7 +206,7 @@
     head_mixed = (
         combined.reshape(span_rows, -1) * jax.nn.silu(out_gate.astype(jnp.float32))
     ).astype(jnp.bfloat16)
-    mixed_out = lax.all_to_all(head_mixed, "tp", split_axis=0, concat_axis=1, tiled=True)
+    mixed_out = task_drive(head_mixed)
     projected = jnp.dot(mixed_out, out_proj, preferred_element_type=jnp.float32)
     residual = (stream.astype(jnp.float32) + normalize(projected) * mix_gain).astype(jnp.bfloat16)
     normed = (normalize(residual.astype(jnp.float32)) * ffn_gain).astype(jnp.bfloat16)

time: 288 us -> 291 us (1.010)
  other arithmetic: 32.2 us -> 35.3 us
    dot_general x14, matrix products: 10.9 us -> 14.2 us  [advance(): jnp.einsum('jco,jcm->com', key_segment, value_segment, precision=TOP_PREC...]
    another operation x8 -> x9, other arithmetic: 6.6 us -> 7.35 us
where the time goes in v1:
time: 291 us; the launch traced here: 289 us
  matrix products  81.8 us (28%)
  waiting for transfers between devices  66.8 us (23%)
  local copies, waits for them, and re-layouts  43.4 us (15%)
  other arithmetic  35.3 us (12%)
  blocking collectives  33.1 us (11%)
  between operations  14.9 us (5%)
  starting transfers between devices  13.3 us (5%)
    all_to_all x1, waiting for transfers between devices, body(): lax.all_to_all(outgoing.reshape(experts, capacity, model_width), 'sp', sp...  36.1 us
    all_gather x1, blocking collectives, carried_in(): gathered = lax.all_gather(packed, axis).astype(jnp.float32)  33.1 us
    dot_general x8, matrix products, feed_forward(): jnp.dot(hidden, down_mat[group * width:(group + 1) * width], preferred_el...  32.2 us
    all_to_all x1, waiting for transfers between devices, body(): lax.all_to_all(routed_done.reshape(experts, capacity, model_width), 'sp',...  22.6 us
    dot_general x16, matrix products, advance(): jnp.einsum('asu,sun->asn', query_segment, carried_state, precision=TOP_PR...  14.9 us
    dot_general x14, matrix products, advance(): jnp.einsum('jco,jcm->com', key_segment, value_segment, precision=TOP_PREC...  14.2 us
    another operation x2, other arithmetic, blockwise(): jnp.cumsum(log_decay.reshape(block_count, BLK, head_count, key_width), ax...  14.1 us
    slice x17, local copies, waits for them, and re-layouts, blockwise(): lax.scan(advance, start_state, (query_in, key_out, value_blocks, block_de...  10.6 us
  transfers between devices with their start and end apart: 9, of which 3 were waited for; matrix products, arithmetic and copies ran while one was open for 54% of the time, Pallas kernels for 0%

profile of v1, /device:TPU:0, one launch (start us, length us, event | category | flops | bytes accessed | tf_op | source)
XLA Modules:
  0.0 288.6 jit_solution(9286686377729508864)
XLA Ops:
  11.9 2.4 reduce-window.14
  17.0 2.4 reduce-window.16
  22.3 3.8 %rev.17 = f32[512,2,128]{0,2,1:T(8,128)S(1)} reverse(f32[512,2,128]{0,2,1:T(8,128)} %bitcast.622), dimensions={0} | reverse | bytes 1048576 | tf_op jit(solution)/shard_map/rev | solution.py:199
  26.1 1.3 fusion.30
  29.0 33.1 %all_gather.28 = bf16[8,258,128]{2,1,0:T(8,128)(2,1)S(1)} all-gather(bf16[1,258,128]{2,1,0:T(8,128)(2,1)S(1)} %pad_maximum_fusion.3), channel_id=1, replica_groups=mesh['sp'=8,'tp'=4] {'sp'}, dimensions={0}, use_global_device_ids=true | all-gather | bytes 594432 | tf_op jit(solution)/shard_map/all_gather | solution.py:32
  72.0 3.3 %rev.18 = f32[512,2,64]{0,2,1:T(8,128)} reverse(f32[512,2,64]{0,2,1:T(8,128)} %get-tuple-element.75), dimensions={0} | reverse | bytes 524288 | tf_op jit(solution)/shard_map/rev | solution.py:197
  75.7 13.0 %fusion.218 = f32[8,64,2,64]{3,0,1,2:T(8,128)S(1)} fusion(f32[8,64,2,64]{3,0,1,2:T(8,128)S(1)} %copy.383), kind=kOutput, calls=%fused_computation.399 | output fusion | flops 4128768 | bytes 524288 | tf_op jit(solution)/shard_map/jit(cumsum)/reduce_window_sum | solution.py:74
  98.0 1.2 fusion.69
  99.3 2.3 copy_multiply_fusion.1
  119.9 1.6 fusion.216
  129.6 1.2 fusion.65
  130.9 2.3 copy_multiply_fusion
  153.5 3.4 %all-to-all-start = ((bf16[4,128,256]{1,2,0:T(8,128)(2,1)}), bf16[4,128,256]{1,2,0:T(8,128)(2,1)S(1)}, u32[]{:S(2)}, u32[]{:S(2)}) async-start(bf16[4,128,256]{1,2,0:T(8,128)(2,1)} %pad_maximum_fusion.2), calls=%async_computation | async-start | bytes 524288 | tf_op jit(solution)/shard_map/all_to_all | solution.py:18
  158.4 4.6 %all-to-all-done = bf16[4,128,256]{1,2,0:T(8,128)(2,1)S(1)} async-done(((bf16[4,128,256]{1,2,0:T(8,128)(2,1)}), bf16[4,128,256]{1,2,0:T(8,128)(2,1)S(1)}, u32[]{:S(2)}, u32[]{:S(2)}) %all-to-all-start) | async-done | bytes 262176 | tf_op jit(solution)/shard_map/all_to_all | solution.py:18
  162.9 3.1 %multiply_reduce_fusion.1 = (f32[128]{0:T(128)S(1)}, f32[128,2048]{1,0:T(8,128)S(1)}) fusion(bf16[128,1024]{0,1:T(8,128)(2,1)S(1)} %bitcast.624, bf16[1024,2048]{1,0:T(8,128)(2,1)} %param.28), kind=kOutput, calls=%fused_computation.110 | convolution fusion | flops 537395072 | bytes 5505536 | tf_op jit(solution)/shard_map/dot_general | solution.py:210
  166.7 1.8 convolution_convert_fusion
  168.5 5.5 %all-to-all-start.1 = ((bf16[8,48,2048]{2,1,0:T(8,128)(2,1)}), bf16[8,48,2048]{2,1,0:T(8,128)(2,1)S(1)}, u32[]{:S(2)}, u32[]{:S(2)}) async-start(bf16[8,48,2048]{2,1,0:T(8,128)(2,1)} %bitcast.616), calls=%async_computation.1 | async-start | bytes 3145728 | tf_op jit(solution)/shard_map/all_to_all | solution.py:217
  174.6 36.1 %all-to-all-done.1 = bf16[8,48,2048]{2,1,0:T(8,128)(2,1)S(1)} async-done(((bf16[8,48,2048]{2,1,0:T(8,128)(2,1)}), bf16[8,48,2048]{2,1,0:T(8,128)(2,1)S(1)}, u32[]{:S(2)}, u32[]{:S(2)}) %all-to-all-start.1) | async-done | bytes 1572896 | tf_op jit(solution)/shard_map/all_to_all | solution.py:217
  210.7 1.9 fusion.39
  214.5 5.0 %fusion.7 = f32[384,2048]{1,0:T(8,128)} fusion(bf16[384,2048]{1,0:T(8,128)(2,1)S(1)} %bitcast.608, bf16[1,1024,2048]{2,1,0:T(8,128)(2,1)} %all-gather.20.cloned.1.call-done, bf16[4,2048,256]{2,1,0:T(8,128)(2,1)} %all-gather.14.cloned.1.call-done, f32[384,256]{1,0:T(8,128)S(1)} %fusion.39), kind=kOutput, calls=%fused_computation.25 | convolution fusion | flops 805896192 | bytes 7208960 | tf_op jit(solution)/shard_map/dot_general | solution.py:121
  219.4 1.8 fusion.37
  221.2 5.0 %fusion.8 = f32[384,2048]{1,0:T(8,128)} fusion(bf16[384,2048]{1,0:T(8,128)(2,1)S(1)} %bitcast.610, bf16[1,1024,2048]{2,1,0:T(8,128)(2,1)} %all-gather.20.cloned.1.call-done, bf16[4,2048,256]{2,1,0:T(8,128)(2,1)} %all-gather.14.cloned.1.call-done, f32[384,256]{1,0:T(8,128)S(1)} %fusion.40), kind=kOutput, calls=%fused_computation.26 | convolution fusion | flops 805896192 | bytes 7208960 | tf_op jit(solution)/shard_map/dot_general | solution.py:121
  226.3 5.0 %fusion.6 = f32[384,2048]{1,0:T(8,128)} fusion(bf16[384,2048]{1,0:T(8,128)(2,1)S(1)} %bitcast.611, bf16[1,1024,2048]{2,1,0:T(8,128)(2,1)} %all-gather.20.cloned.1.call-done, bf16[4,2048,256]{2,1,0:T(8,128)(2,1)} %all-gather.14.cloned.1.call-done, f32[384,256]{1,0:T(8,128)S(1)} %fusion.38), kind=kOutput, calls=%fused_computation.24 | convolution fusion | flops 805896192 | bytes 7208960 | tf_op jit(solution)/shard_map/dot_general | solution.py:121
  231.2 7.3 %add_convert_fusion = bf16[384,2048]{1,0:T(8,128)(2,1)} fusion(f32[384,2048]{1,0:T(8,128)} %fusion.6, f32[384,2048]{1,0:T(8,128)} %fusion.8, f32[384,2048]{1,0:T(8,128)} %fusion.7, bf16[1,1024,2048]{2,1,0:T(8,128)(2,1)} %all-gather.20.cloned.1.call-done, bf16[384,2048]{1,0:T(8,128)(2,1)S(1)} %bitcast.612, ...), kind=kOutput, calls=%fused_computation | convolution fusion | flops 809041920 | bytes 15073280 | tf_op jit(solution)/shard_map/dot_general | solution.py:121
  238.6 4.0 %all-to-all-start.2 = ((bf16[8,48,2048]{2,1,0:T(8,128)(2,1)}), bf16[8,48,2048]{2,1,0:T(8,128)(2,1)S(1)}, u32[]{:S(2)}, u32[]{:S(2)}) async-start(bf16[8,48,2048]{2,1,0:T(8,128)(2,1)} %bitcast.615), calls=%async_computation.2 | async-start | bytes 3145728 | tf_op jit(solution)/shard_map/all_to_all | solution.py:228
  242.7 1.5 fusion.48
  244.3 1.4 fusion.53
  247.1 1.8 fusion.31
  248.9 2.8 convolution_add_fusion.4
  251.7 3.1 %convolution_add_fusion.3 = f32[128,2048]{1,0:T(8,128)} fusion(f32[128,2048]{1,0:T(8,128)} %convolution_add_fusion.4, bf16[512,2048]{1,0:T(8,128)(2,1)} %all-gather.10.cloned.1.call-done, bf16[8192,128]{1,0:T(8,128)(2,1)} %all-gather.18.cloned.1.call-done, f32[128,128]{1,0:T(8,128)S(1)} %fusion.53, bf16[128,2048]{1,0:T(8,128)(2,1)S(1)} %get-tuple-element.6, ...), kind=kOutput, calls=%fused_computation.5 | convolution fusion | flops 135626752 | bytes 3744256 | tf_op jit(solution)/shard_map/dot_general | solution.py:121
  254.8 2.1 convolution_add_fusion.2
  257.0 22.6 %all-to-all-done.2 = bf16[8,48,2048]{2,1,0:T(8,128)(2,1)S(1)} async-done(((bf16[8,48,2048]{2,1,0:T(8,128)(2,1)}), bf16[8,48,2048]{2,1,0:T(8,128)(2,1)S(1)}, u32[]{:S(2)}, u32[]{:S(2)}) %all-to-all-start.2) | async-done | bytes 1572896 | tf_op jit(solution)/shard_map/all_to_all | solution.py:228
  (285 shorter events, 85.9 us)
Async XLA Ops:
  6.5 204.2 %all-gather.12.cloned.1.call-start = ((), (), s32[]{:S(2)}) async-start(), calls=%async_computation.4 | async-start | bytes 5242880 | tf_op jit(solution)/shard_map/all_gather | solution.py:169
  7.3 207.2 %all-gather.14.cloned.1.call-start = ((), (), s32[]{:S(2)}) async-start(), calls=%async_computation.5 | async-start | bytes 5242880 | tf_op jit(solution)/shard_map/all_gather | solution.py:170
  8.0 206.4 %all-gather.20.cloned.1.call-start = ((), (), s32[]{:S(2)}) async-start(), calls=%async_computation.8 | async-start | bytes 5242880 | tf_op jit(solution)/shard_map/all_gather | solution.py:171
  8.7 234.0 %all-gather.16.cloned.1.call-start = ((), (), s32[]{:S(2)}) async-start(), calls=%async_computation.6 | async-start | bytes 2621440 | tf_op jit(solution)/shard_map/all_gather | solution.py:172
  98.0 8.1 %copy-start.30 = (bf16[8,2,8,128]{3,2,1,0:T(8,128)(2,1)S(1)}, bf16[8,2,8,128]{3,2,1,0:T(8,128)(2,1)}, u32[]{:S(2)}) copy-start(bf16[8,2,8,128]{3,2,1,0:T(8,128)(2,1)} %get-tuple-element.26) | copy-start | bytes 98308
  99.2 8.9 %copy-start.29 = (bf16[8,2,8,128]{3,2,1,0:T(8,128)(2,1)S(1)}, bf16[8,2,8,128]{3,2,1,0:T(8,128)(2,1)}, u32[]{:S(2)}) copy-start(bf16[8,2,8,128]{3,2,1,0:T(8,128)(2,1)} %get-tuple-element.25) | copy-start | bytes 98308
  99.3 11.0 %copy-start.28 = (bf16[8,2,8,128]{3,2,1,0:T(8,128)(2,1)S(1)}, bf16[8,2,8,128]{3,2,1,0:T(8,128)(2,1)}, u32[]{:S(2)}) copy-start(bf16[8,2,8,128]{3,2,1,0:T(8,128)(2,1)} %get-tuple-element.24) | copy-start | bytes 98308
  99.3 13.0 %copy-start.27 = (bf16[8,2,8,128]{3,2,1,0:T(8,128)(2,1)S(1)}, bf16[8,2,8,128]{3,2,1,0:T(8,128)(2,1)}, u32[]{:S(2)}) copy-start(bf16[8,2,8,128]{3,2,1,0:T(8,128)(2,1)} %get-tuple-element.29) | copy-start | bytes 98308
  101.6 12.8 %copy-start.26 = (bf16[8,2,8,128]{3,2,1,0:T(8,128)(2,1)S(1)}, bf16[8,2,8,128]{3,2,1,0:T(8,128)(2,1)}, u32[]{:S(2)}) copy-start(bf16[8,2,8,128]{3,2,1,0:T(8,128)(2,1)} %get-tuple-element.23) | copy-start | bytes 98308
  101.6 14.9 %copy-start.7 = (f32[8,64,2,64]{3,0,1,2:T(8,128)S(1)}, f32[8,64,2,64]{3,0,1,2:T(8,128)}, u32[]{:S(2)}) copy-start(f32[8,64,2,64]{3,0,1,2:T(8,128)} %copy.352) | copy-start | bytes 786436
  101.6 14.9 %copy-start.9 = (f32[8,64,2,64]{3,0,1,2:T(8,128)S(1)}, f32[8,64,2,64]{3,0,1,2:T(8,128)}, u32[]{:S(2)}) copy-start(f32[8,64,2,64]{3,0,1,2:T(8,128)} %copy.354) | copy-start | bytes 786436
  118.1 9.9 %copy-start.13 = (f32[64,256]{0,1:T(8,128)S(1)}, f32[64,256]{0,1:T(8,128)}, u32[]{:S(2)}) copy-start(f32[64,256]{0,1:T(8,128)} %get-tuple-element.32) | copy-start | bytes 196612
  118.1 10.6 %copy-start.12 = (f32[64,256]{0,1:T(8,128)S(1)}, f32[64,256]{0,1:T(8,128)}, u32[]{:S(2)}) copy-start(f32[64,256]{0,1:T(8,128)} %get-tuple-element.31) | copy-start | bytes 196612
  129.6 7.0 %copy-start.23 = (f32[64,2,128]{2,0,1:T(8,128)S(1)}, f32[64,2,128]{2,0,1:T(8,128)}, u32[]{:S(2)}) copy-start(f32[64,2,128]{2,0,1:T(8,128)} %slice.534) | copy-start | bytes 196612
  129.6 7.0 %copy-start.47 = (f32[1,2,64]{2,0,1:T(1,128)S(1)}, f32[1,2,64]{2,0,1:T(1,128)}, u32[]{:S(2)}) copy-start(f32[1,2,64]{2,0,1:T(1,128)} %get-tuple-element.67) | copy-start | bytes 1540
  129.6 9.0 %copy-start.22 = (f32[64,2,128]{2,0,1:T(8,128)S(1)}, f32[64,2,128]{2,0,1:T(8,128)}, u32[]{:S(2)}) copy-start(f32[64,2,128]{2,0,1:T(8,128)} %slice.540) | copy-start | bytes 196612
  129.6 9.0 %copy-start.46 = (f32[1,2,64]{2,0,1:T(1,128)S(1)}, f32[1,2,64]{2,0,1:T(1,128)}, u32[]{:S(2)}) copy-start(f32[1,2,64]{2,0,1:T(1,128)} %get-tuple-element.66) | copy-start | bytes 1540
  130.9 9.9 %copy-start.21 = (f32[64,2,128]{2,0,1:T(8,128)S(1)}, f32[64,2,128]{2,0,1:T(8,128)}, u32[]{:S(2)}) copy-start(f32[64,2,128]{2,0,1:T(8,128)} %slice.546) | copy-start | bytes 196612
  130.9 9.9 %copy-start.45 = (f32[1,2,64]{2,0,1:T(1,128)S(1)}, f32[1,2,64]{2,0,1:T(1,128)}, u32[]{:S(2)}) copy-start(f32[1,2,64]{2,0,1:T(1,128)} %get-tuple-element.65) | copy-start | bytes 1540
  130.9 12.0 %copy-start.20 = (f32[64,2,128]{2,0,1:T(8,128)S(1)}, f32[64,2,128]{2,0,1:T(8,128)}, u32[]{:S(2)}) copy-start(f32[64,2,128]{2,0,1:T(8,128)} %slice.552) | copy-start | bytes 196612
  130.9 12.0 %copy-start.44 = (f32[1,2,64]{2,0,1:T(1,128)S(1)}, f32[1,2,64]{2,0,1:T(1,128)}, u32[]{:S(2)}) copy-start(f32[1,2,64]{2,0,1:T(1,128)} %get-tuple-element.64) | copy-start | bytes 1540
  130.9 14.1 %copy-start.19 = (f32[64,2,128]{2,0,1:T(8,128)S(1)}, f32[64,2,128]{2,0,1:T(8,128)}, u32[]{:S(2)}) copy-start(f32[64,2,128]{2,0,1:T(8,128)} %slice.558) | copy-start | bytes 196612
  130.9 14.1 %copy-start.43 = (f32[1,2,64]{2,0,1:T(1,128)S(1)}, f32[1,2,64]{2,0,1:T(1,128)}, u32[]{:S(2)}) copy-start(f32[1,2,64]{2,0,1:T(1,128)} %get-tuple-element.63) | copy-start | bytes 1540
  133.2 13.9 %copy-start.42 = (f32[1,2,64]{2,0,1:T(1,128)S(1)}, f32[1,2,64]{2,0,1:T(1,128)}, u32[]{:S(2)}) copy-start(f32[1,2,64]{2,0,1:T(1,128)} %get-tuple-element.62) | copy-start | bytes 1540
  133.2 16.0 %copy-start.6 = (f32[8,64,2,64]{3,0,1,2:T(8,128)S(1)}, f32[8,64,2,64]{3,0,1,2:T(8,128)}, u32[]{:S(2)}) copy-start(f32[8,64,2,64]{3,0,1,2:T(8,128)} %copy.384) | copy-start | bytes 786436
  133.2 16.0 %copy-start.8 = (f32[8,64,2,64]{3,0,1,2:T(8,128)S(1)}, f32[8,64,2,64]{3,0,1,2:T(8,128)}, u32[]{:S(2)}) copy-start(f32[8,64,2,64]{3,0,1,2:T(8,128)} %copy.385) | copy-start | bytes 786436
  133.2 16.0 %copy-start.35 = (f32[8,2,64]{2,0,1:T(8,128)S(1)}, f32[8,2,64]{2,0,1:T(8,128)}, u32[]{:S(2)}) copy-start(f32[8,2,64]{2,0,1:T(8,128)} %get-tuple-element.13) | copy-start | bytes 12292
  153.5 9.4 %all-to-all-start = ((bf16[4,128,256]{1,2,0:T(8,128)(2,1)}), bf16[4,128,256]{1,2,0:T(8,128)(2,1)S(1)}, u32[]{:S(2)}, u32[]{:S(2)}) async-start(bf16[4,128,256]{1,2,0:T(8,128)(2,1)} %pad_maximum_fusion.2), calls=%async_computation | async-start | bytes 524288 | tf_op jit(solution)/shard_map/all_to_all | solution.py:18
  156.9 90.1 %all-gather.10.cloned.1.call-start = ((), (), s32[]{:S(2)}) async-start(), calls=%async_computation.3 | async-start | bytes 2621440 | tf_op jit(solution)/shard_map/all_gather | solution.py:174
  168.5 42.2 %all-to-all-start.1 = ((bf16[8,48,2048]{2,1,0:T(8,128)(2,1)}), bf16[8,48,2048]{2,1,0:T(8,128)(2,1)S(1)}, u32[]{:S(2)}, u32[]{:S(2)}) async-start(bf16[8,48,2048]{2,1,0:T(8,128)(2,1)} %bitcast.616), calls=%async_computation.1 | async-start | bytes 3145728 | tf_op jit(solution)/shard_map/all_to_all | solution.py:217
  174.0 73.1 %all-gather.18.cloned.1.call-start = ((), (), s32[]{:S(2)}) async-start(), calls=%async_computation.7 | async-start | bytes 2621440 | tf_op jit(solution)/shard_map/all_gather | solution.py:173
  238.6 41.0 %all-to-all-start.2 = ((bf16[8,48,2048]{2,1,0:T(8,128)(2,1)}), bf16[8,48,2048]{2,1,0:T(8,128)(2,1)S(1)}, u32[]{:S(2)}, u32[]{:S(2)}) async-start(bf16[8,48,2048]{2,1,0:T(8,128)(2,1)} %bitcast.615), calls=%async_computation.2 | async-start | bytes 3145728 | tf_op jit(solution)/shard_map/all_to_all | solution.py:228
  (32 other events, 116.7 us)
Sparse Core Ops, SparseCore 0:
  8.9 37.2 all-gather.11
  47.7 34.4 all-gather.13
  83.8 34.4 all-gather.19
  119.7 22.5 all-gather.15
  159.0 23.9 all-gather.9
  184.4 22.5 all-gather.17
